TPU v7x, 32 devices: a whole 2x2x4 slice. The times are simulated.
32 devices in a mesh: sp: 16 (over z, y, core), tp: 2 (over x).
Axes of the slice: x: 2, y: 2, z: 4, core: 2. Of those that a mesh axis runs over, the one named last changes fastest.
Arguments:
- residual: bfloat16 [2048, 2048], P(('sp', 'tp')), may hold values from -6 to 6
- q_small: bfloat16 [2048, 1024], P('sp', 'tp'), may hold values from -6 to 6
- k_small: bfloat16 [2048, 1024], P('sp', 'tp'), may hold values from -6 to 6
- v_small: bfloat16 [2048, 1024], P('sp', 'tp'), may hold values from -6 to 6
- q_large: bfloat16 [2048, 1024], P('sp', 'tp'), may hold values from -6 to 6
- k_large: bfloat16 [2048, 1024], P('sp', 'tp'), may hold values from -6 to 6
- v_large: bfloat16 [2048, 1024], P('sp', 'tp'), may hold values from -6 to 6
- forget_small: float32 [2048, 16], P('sp', 'tp'), may hold values from 0 to 20
- forget_large: float32 [2048, 8], P('sp', 'tp'), may hold values from 0 to 20
- w_out_small: bfloat16 [1024, 2048], P('tp'), may hold values from -0.125 to 0.125
- w_out_large: bfloat16 [1024, 2048], P('tp'), may hold values from -0.125 to 0.125
- norm_gain: float32 [2048], replicated, may hold values from 0.1 to 1.9
- w_gate: bfloat16 [2048, 4096], P('sp', 'tp'), may hold values from -0.125 to 0.125
- w_up: bfloat16 [2048, 4096], P('sp', 'tp'), may hold values from -0.125 to 0.125
- conv_gate: float32 [3, 4096], P(None, 'tp'), may hold values from -3 to 3
- conv_up: float32 [3, 4096], P(None, 'tp'), may hold values from -3 to 3
- w_down: bfloat16 [4096, 2048], P('tp', 'sp'), may hold values from -0.09375 to 0.09375
Outputs:
- mixed: bfloat16 [2048, 2048], P(('sp', 'tp'))
All inputs are finite; a program needn't handle non-finite values.
Results may differ from a plain program's by a relative error of at most 0.015.
Values may be sent and summed in bfloat16 or wider, within the bound.
A program may use at most 64 MiB of HBM per device.

v0:
```python
import jax
import jax.numpy as jnp
from jax import lax
from jax.sharding import PartitionSpec as P

EPS = 1e-06
NEG = -1e30


def from_behind(block, axis, distance):
    devices = range(lax.axis_size(axis))
    route = [(i - distance, i) for i in devices if i - distance in devices]
    return lax.ppermute(block, axis, route)


def globalize(part, rows):
    heads = part.shape[1]
    blocks = part.reshape(-1, rows, heads)
    totals = blocks[:, -1, :]
    before = jnp.cumsum(totals, axis=0) - totals
    return (blocks + before[:, None, :]).reshape(part.shape)


def attend(carry, keys, values, queries, cum_own, cum_every, qpos):
    top, denom, accum = carry
    count = keys.shape[0]
    heads = queries.shape[1]
    size = queries.shape[2]
    keys = keys.reshape(count, heads, size)
    values = values.reshape(count, heads, size)
    kpos = jnp.arange(count, dtype=jnp.int32)
    scores = jnp.einsum(
        "qhd,khd->qhk", queries, keys, preferred_element_type=jnp.float32
    ) * size ** (-0.5)
    scores = scores + cum_own[:, :, None] - cum_every.T[None, :, :]
    keep = (kpos[None, :] <= qpos[:, None])[:, None, :]
    scores = jnp.where(keep, scores, NEG)
    new_top = jnp.maximum(top, jnp.max(scores, axis=-1))
    weights = jnp.where(keep, jnp.exp(scores - new_top[:, :, None]), 0.0)
    denom = jnp.sum(weights, axis=-1)
    accum = jnp.einsum(
        "qhk,khd->qhd", weights.astype(jnp.bfloat16), values, preferred_element_type=jnp.float32
    )
    return (new_top, denom, accum)


def finish(carry):
    top, denom, accum = carry
    attended = accum / denom[:, :, None]
    normed = attended * lax.rsqrt(jnp.mean(attended * attended, axis=-1, keepdims=True) + EPS)
    return normed.astype(jnp.bfloat16).reshape(attended.shape[0], -1)


def empty_carry(rows, heads, size):
    return (
        jnp.full((rows, heads), NEG, jnp.float32),
        jnp.zeros((rows, heads), jnp.float32),
        jnp.zeros((rows, heads, size), jnp.float32),
    )


def body(
    residual,
    q_small,
    k_small,
    v_small,
    q_large,
    k_large,
    v_large,
    forget_small,
    forget_large,
    w_out_small,
    w_out_large,
    norm_gain,
    w_gate,
    w_up,
    conv_gate,
    conv_up,
    w_down,
):
    rows = q_small.shape[0]
    offset = lax.axis_index("sp") * rows
    qpos = offset + jnp.arange(rows, dtype=jnp.int32)
    gathered = (
        lax.all_gather(w_gate, "sp", axis=0, tiled=True),
        lax.all_gather(w_up, "sp", axis=0, tiled=True),
        lax.all_gather(w_down, "sp", axis=1, tiled=True),
    )
    local_small = jnp.cumsum(jax.nn.log_sigmoid(forget_small), axis=0)
    local_large = jnp.cumsum(jax.nn.log_sigmoid(forget_large), axis=0)
    part_small, part_large = (
        lax.all_gather(local_small, "sp", axis=0, tiled=True),
        lax.all_gather(local_large, "sp", axis=0, tiled=True),
    )
    every_small = globalize(part_small, rows)
    every_large = globalize(part_large, rows)
    cum_small = lax.dynamic_slice_in_dim(every_small, offset, rows, 0)
    cum_large = lax.dynamic_slice_in_dim(every_large, offset, rows, 0)
    heads_small = forget_small.shape[1]
    heads_large = forget_large.shape[1]
    queries_small = q_small.reshape(rows, heads_small, -1)
    queries_large = q_large.reshape(rows, heads_large, -1)
    start_carry = (
        empty_carry(rows, heads_small, queries_small.shape[2]),
        empty_carry(rows, heads_large, queries_large.shape[2]),
    )
    keys_s = lax.all_gather(k_small, "sp", axis=0, tiled=True)
    values_s = lax.all_gather(v_small, "sp", axis=0, tiled=True)
    keys_l = lax.all_gather(k_large, "sp", axis=0, tiled=True)
    values_l = lax.all_gather(v_large, "sp", axis=0, tiled=True)
    small = attend(start_carry[0], keys_s, values_s, queries_small, cum_small, every_small, qpos)
    large = attend(start_carry[1], keys_l, values_l, queries_large, cum_large, every_large, qpos)
    normed_small = finish(small)
    normed_large = finish(large)
    first_part = jnp.dot(normed_small, w_out_small, preferred_element_type=jnp.float32)
    projected = lax.psum_scatter(
        (
            first_part + jnp.dot(normed_large, w_out_large, preferred_element_type=jnp.float32)
        ).astype(jnp.bfloat16),
        "tp",
        scatter_dimension=0,
        tiled=True,
    ).astype(jnp.float32)
    first = residual.astype(jnp.float32) + projected
    normal = (
        first * lax.rsqrt(jnp.mean(first * first, axis=-1, keepdims=True) + EPS) * norm_gain
    ).astype(jnp.bfloat16)
    gate_full, up_full, down_full = gathered
    piece = lax.all_gather(normal, "tp", axis=0, tiled=True)
    gate_part = jnp.dot(piece, gate_full, preferred_element_type=jnp.float32).astype(jnp.bfloat16)
    up_part = jnp.dot(piece, up_full, preferred_element_type=jnp.float32).astype(jnp.bfloat16)
    both = jnp.concatenate([gate_part, up_part], axis=1)
    width = both.shape[0]
    rim = from_behind(both[width - 2 :], "sp", 1)
    extended = jnp.concatenate([rim, both], axis=0).astype(jnp.float32)
    taps = jnp.concatenate([conv_gate, conv_up], axis=1)
    conv = (
        taps[0] * extended[0:width]
        + taps[1] * extended[1 : width + 1]
        + taps[2] * extended[2 : width + 2]
    )
    half = gate_full.shape[1]
    hidden = (jax.nn.silu(conv[:, :half]) * conv[:, half:]).astype(jnp.bfloat16)
    mixed = first + lax.psum_scatter(
        jnp.dot(hidden, down_full, preferred_element_type=jnp.float32).astype(jnp.bfloat16),
        "tp",
        scatter_dimension=0,
        tiled=True,
    ).astype(jnp.float32)
    return mixed.astype(jnp.bfloat16)


def solution(mesh):
    placed = (
        P(("sp", "tp"), None),
        P("sp", "tp"),
        P("sp", "tp"),
        P("sp", "tp"),
        P("sp", "tp"),
        P("sp", "tp"),
        P("sp", "tp"),
        P("sp", "tp"),
        P("sp", "tp"),
        P("tp", None),
        P("tp", None),
        P(),
        P("sp", "tp"),
        P("sp", "tp"),
        P(None, "tp"),
        P(None, "tp"),
        P("tp", "sp"),
    )
    return jax.shard_map(
        body, mesh=mesh, in_specs=placed, out_specs=P(("sp", "tp"), None), check_vma=False
    )
```

profile of v0, /device:TPU:0, one launch (start us, length us, event | category | flops | bytes accessed | tf_op | source)
XLA Modules:
  0.0 472.0 jit_solution(16428870450614130786)
XLA Ops:
  6.5 0.7 all-gather.14.cloned.1.call-update
  7.3 0.0 all-gather.8.cloned.1.call-start
  7.3 0.7 all-gather.8.cloned.1.call-update
  8.0 0.0 all-gather.12.cloned.1.call-start
  8.1 1.7 copy.44
  9.7 0.0 all-gather.10.cloned.1.call-start
  9.8 0.5 all-gather.10.cloned.1.call-update
  10.3 0.0 reduce-scatter.3.cloned.1.call-start
  10.4 0.7 fusion.40
  11.1 0.1 copy.47
  11.2 0.2 reduce_window_sum.46
  11.4 27.1 %all_gather.34 = f32[2048,4]{1,0:T(8,128)S(1)} all-gather(f32[128,4]{1,0:T(8,128)S(1)} %reduce_window_sum.46), channel_id=1, replica_groups=mesh['sp'=16,'tp'=2] {'sp'}, dimensions={0}, use_global_device_ids=true | all-gather | bytes 34816 | tf_op jit(solution)/shard_map/all_gather | solution.py:93
  38.5 0.1 bitcast_add_fusion.2
  38.6 0.1 copy.37
  38.7 0.2 reduce_window_sum.44
  38.8 24.5 %all_gather.31 = f32[2048,8]{1,0:T(8,128)S(1)} all-gather(f32[128,8]{1,0:T(8,128)S(1)} %reduce_window_sum.44), channel_id=1, replica_groups=mesh['sp'=16,'tp'=2] {'sp'}, dimensions={0}, use_global_device_ids=true | all-gather | bytes 69632 | tf_op jit(solution)/shard_map/all_gather | solution.py:92
  63.4 1.1 bitcast_add_fusion.3
  64.4 0.8 constant_dynamic-slice_fusion.1
  65.3 0.1 copy.50
  65.4 0.3 copy.51
  65.7 0.1 copy.40
  65.7 1.6 copy.41
  67.3 0.1 copy.36
  67.4 0.2 iota_compare_fusion
  67.7 4.0 copy.52
  71.7 31.4 %all-gather.8.cloned.1.call-done = bf16[2048,512]{1,0:T(8,128)(2,1)} async-done(((bf16[128,512]{1,0:T(8,128)(2,1)}), bf16[2048,512]{1,0:T(8,128)(2,1)}) %all-gather.8.cloned.1.call-update) | async-done | bytes 2097168 | tf_op jit(solution)/shard_map/all_gather | solution.py:107
  103.0 4.0 copy.35
  107.0 38.0 %all-gather.12.cloned.1.call-done = bf16[2048,512]{0,1:T(8,128)(2,1)} async-done(((bf16[128,512]{0,1:T(8,128)(2,1)}), bf16[2048,512]{0,1:T(8,128)(2,1)}) %all-gather.12.cloned.1.call-update) | async-done | bytes 2097168 | tf_op jit(solution)/shard_map/all_gather | solution.py:109
  145.0 3.7 fusion.47
  148.7 0.8 fusion.10
  149.5 0.8 copy-done.7
  150.3 1.2 multiply_reduce_fusion.1
  151.4 0.4 copy-done.6
  151.9 3.4 fusion.4
  155.3 3.2 copy-done.2
  158.5 3.1 fusion.2
  161.6 26.0 %all-gather.10.cloned.1.call-done = bf16[2048,512]{1,0:T(8,128)(2,1)} async-done(((bf16[128,512]{1,0:T(8,128)(2,1)}), bf16[2048,512]{1,0:T(8,128)(2,1)}) %all-gather.10.cloned.1.call-update) | async-done | bytes 2097168 | tf_op jit(solution)/shard_map/all_gather | solution.py:108
  187.6 3.9 copy.42
  191.5 6.6 %multiply_reduce_fusion.2 = (f32[128,8]{0,1:T(8,128)S(1)}, f32[128,8,64]{0,2,1:T(8,128)S(1)}) fusion(f32[128,8]{0,1:T(8,128)S(1)} %fusion.2, bf16[2048,8,64]{0,2,1:T(8,128)(2,1)} %bitcast.82, f32[8,2048,128]{2,1,0:T(8,128)} %copy-done.2, f32[128,8]{0,1:T(8,128)S(1)} %broadcast_maximum_fusion, f32[8,2048]{1,0:T(8,128)S(1)} %copy.41, f32[128,8]{0,1:T(8,128)S(1)} %copy.40, ...), kind=kOutput, calls=%fused_computation.49 | convolution fusion | flops 283311104 | bytes 11091968 | tf_op jit(solution)/shard_map/qhk,khd->qhd/dot_general | solution.py:41
  198.3 0.5 fusion.48
  198.8 1.0 copy-done.5
  199.7 1.3 fusion.12
  201.1 0.0 all-gather.18.cloned.1.call-start
  201.1 0.5 all-gather.18.cloned.1.call-update
  201.6 0.0 all-gather.16.cloned.1.call-start
  201.7 0.7 all-gather.16.cloned.1.call-update
  202.4 0.7 all-gather.20.cloned.1.call-update
  203.1 0.0 reduce-scatter.5.cloned.1.call-start
  203.2 11.3 %reduce-scatter.3.cloned.1.call-done = bf16[64,2048]{1,0:T(8,128)(2,1)} async-done(((bf16[128,2048]{1,0:T(8,128)(2,1)}), bf16[64,2048]{1,0:T(8,128)(2,1)}) %reduce-scatter.3.cloned.1.call-update) | async-done | bytes 262160 | tf_op jit(solution)/shard_map/reduce_scatter | solution.py:116
  214.6 1.1 multiply_reduce_fusion
  215.7 1.1 multiply_convert_fusion
  216.8 8.7 %all_gather.36 = bf16[128,2048]{1,0:T(8,128)(2,1)S(1)} all-gather(bf16[64,2048]{1,0:T(8,128)(2,1)S(1)} %multiply_convert_fusion), channel_id=1, replica_groups=mesh['sp'=16,'tp'=2] {'tp'}, dimensions={0}, use_global_device_ids=true | all-gather | bytes 786432 | tf_op jit(solution)/shard_map/all_gather | solution.py:129
  225.5 65.4 %all-gather.18.cloned.1.call-done = bf16[2048,2048]{1,0:T(8,128)(2,1)} async-done(((bf16[128,2048]{1,0:T(8,128)(2,1)}), bf16[2048,2048]{1,0:T(8,128)(2,1)}) %all-gather.18.cloned.1.call-update) | async-done | bytes 8388624 | tf_op jit(solution)/shard_map/all_gather | solution.py:86
  290.9 4.6 convolution_convert_fusion.1
  295.6 70.4 %all-gather.16.cloned.1.call-done = bf16[2048,2048]{1,0:T(8,128)(2,1)} async-done(((bf16[128,2048]{1,0:T(8,128)(2,1)}), bf16[2048,2048]{1,0:T(8,128)(2,1)}) %all-gather.16.cloned.1.call-update) | async-done | bytes 8388624 | tf_op jit(solution)/shard_map/all_gather | solution.py:85
  366.0 4.6 convolution_convert_fusion.2
  370.7 2.2 collective-permute-start
  372.9 0.8 collective-permute-done
  373.6 0.3 maximum_convert_fusion
  373.9 2.0 fusion.15
  375.9 68.5 %all-gather.20.cloned.1.call-done = bf16[2048,2048]{1,0:T(8,128)(2,1)} async-done(((bf16[2048,128]{1,0:T(8,128)(2,1)}), bf16[2048,2048]{1,0:T(8,128)(2,1)}) %all-gather.20.cloned.1.call-update) | async-done | bytes 8388624 | tf_op jit(solution)/shard_map/all_gather | solution.py:87
  444.5 6.3 %convolution_convert_fusion = bf16[128,2048]{1,0:T(8,128)(2,1)} fusion(bf16[2048,2048]{1,0:T(8,128)(2,1)} %all-gather.20.cloned.1.call-done, f32[128,4096]{1,0:T(8,128)} %fusion.15), kind=kOutput, calls=%fused_computation.16 | convolution fusion | flops 1075576832 | bytes 11010048 | tf_op jit(solution)/shard_map/dot_general | solution.py:145
  450.8 13.0 %reduce-scatter.5.cloned.1.call-done = bf16[64,2048]{1,0:T(8,128)(2,1)} async-done(((bf16[128,2048]{1,0:T(8,128)(2,1)}), bf16[64,2048]{1,0:T(8,128)(2,1)}) %reduce-scatter.5.cloned.1.call-update) | async-done | bytes 262160 | tf_op jit(solution)/shard_map/reduce_scatter | solution.py:144
  463.8 1.7 add_convert_fusion
  (46 shorter events, 0.4 us)
Async XLA Ops:
  6.5 191.7 %copy-start = (bf16[512,2048]{1,0:T(8,128)(2,1)S(1)}, bf16[512,2048]{1,0:T(8,128)(2,1)}, u32[]{:S(2)}) copy-start(bf16[512,2048]{1,0:T(8,128)(2,1)} %param.26) | copy-start | bytes 6291460
  6.5 32.0 %copy-start.12 = (f32[128,8]{0,1:T(8,128)S(1)}, f32[128,8]{0,1:T(8,128)}, u32[]{:S(2)}) copy-start(f32[128,8]{0,1:T(8,128)} %param.24) | copy-start | bytes 12292
  6.5 61.1 %all-gather.14.cloned.1.call-start = ((), (), s32[]{:S(2)}) async-start(), calls=%async_computation.5 | async-start | bytes 2228224 | tf_op jit(solution)/shard_map/all_gather | solution.py:110
  7.3 95.8 %all-gather.8.cloned.1.call-start = ((), (), s32[]{:S(2)}) async-start(), calls=%async_computation.2 | async-start | bytes 2228224 | tf_op jit(solution)/shard_map/all_gather | solution.py:107
  8.0 137.0 %all-gather.12.cloned.1.call-start = ((), (), s32[]{:S(2)}) async-start(), calls=%async_computation.4 | async-start | bytes 2228224 | tf_op jit(solution)/shard_map/all_gather | solution.py:109
  9.7 177.8 %all-gather.10.cloned.1.call-start = ((), (), s32[]{:S(2)}) async-start(), calls=%async_computation.3 | async-start | bytes 2228224 | tf_op jit(solution)/shard_map/all_gather | solution.py:108
  10.3 204.2 %reduce-scatter.3.cloned.1.call-start = ((), (), s32[]{:S(2)}) async-start(), calls=%async_computation.6 | async-start | bytes 786432 | tf_op jit(solution)/shard_map/reduce_scatter | solution.py:116
  38.4 28.9 %copy-start.8 = (bf16[128,512]{1,0:T(8,128)(2,1)S(1)}, bf16[128,512]{1,0:T(8,128)(2,1)}, u32[]{:S(2)}) copy-start(bf16[128,512]{1,0:T(8,128)(2,1)} %param.18) | copy-start | bytes 393220
  67.6 77.4 %copy-start.13 = (bf16[128,512]{1,0:T(8,128)(2,1)S(1)}, bf16[128,512]{1,0:T(8,128)(2,1)}, u32[]{:S(2)}) copy-start(bf16[128,512]{1,0:T(8,128)(2,1)} %param.21) | copy-start | bytes 393220
  148.7 1.6 copy-start.7
  150.3 1.6 copy-start.6
  155.2 3.2 copy-start.2
  198.1 1.6 copy-start.5
  198.2 5.0 %copy-start.9 = (f32[3,2048]{1,0:T(4,128)S(1)}, f32[3,2048]{1,0:T(4,128)}, u32[]{:S(2)}) copy-start(f32[3,2048]{1,0:T(4,128)} %param.31) | copy-start | bytes 73732
  198.2 5.0 %copy-start.10 = (f32[3,2048]{1,0:T(4,128)S(1)}, f32[3,2048]{1,0:T(4,128)}, u32[]{:S(2)}) copy-start(f32[3,2048]{1,0:T(4,128)} %param.32) | copy-start | bytes 73732
  198.3 16.3 %copy-start.3 = (bf16[64,2048]{1,0:T(8,128)(2,1)S(1)}, bf16[64,2048]{1,0:T(8,128)(2,1)}, u32[]{:S(2)}) copy-start(bf16[64,2048]{1,0:T(8,128)(2,1)} %param.17) | copy-start | bytes 786436
  198.3 17.5 %copy-start.11 = (f32[2048]{0:T(1024)S(1)}, f32[2048]{0:T(1024)}, u32[]{:S(2)}) copy-start(f32[2048]{0:T(1024)} %param.28) | copy-start | bytes 24580
  201.1 89.8 %all-gather.18.cloned.1.call-start = ((), (), s32[]{:S(2)}) async-start(), calls=%async_computation.8 | async-start | bytes 8912896 | tf_op jit(solution)/shard_map/all_gather | solution.py:86
  201.6 164.3 %all-gather.16.cloned.1.call-start = ((), (), s32[]{:S(2)}) async-start(), calls=%async_computation.7 | async-start | bytes 8912896 | tf_op jit(solution)/shard_map/all_gather | solution.py:85
  202.4 242.1 %all-gather.20.cloned.1.call-start = ((), (), s32[]{:S(2)}) async-start(), calls=%async_computation.9 | async-start | bytes 8912896 | tf_op jit(solution)/shard_map/all_gather | solution.py:87
  203.1 260.6 %reduce-scatter.5.cloned.1.call-start = ((), (), s32[]{:S(2)}) async-start(), calls=%async_computation.10 | async-start | bytes 786432 | tf_op jit(solution)/shard_map/reduce_scatter | solution.py:144
  370.7 3.0 collective-permute-start
  375.9 87.8 %copy-start.4 = (bf16[64,2048]{1,0:T(8,128)(2,1)S(1)}, bf16[64,2048]{1,0:T(8,128)(2,1)}, u32[]{:S(2)}) copy-start(bf16[64,2048]{1,0:T(8,128)(2,1)} %reduce-scatter.3.cloned.1.call-done) | copy-start | bytes 786436
  444.5 21.0 %copy-start.1 = (bf16[512,2048]{1,0:T(8,128)(2,1)S(1)}, bf16[512,2048]{1,0:T(8,128)(2,1)}, u32[]{:S(2)}) copy-start(bf16[512,2048]{1,0:T(8,128)(2,1)} %param.26) | copy-start | bytes 6291460
Sparse Core Ops, SparseCore 0:
  9.5 49.7 all-gather.13
  61.4 41.5 all-gather.7
  105.2 39.7 all-gather.11
  147.0 40.5 all-gather.9
  201.2 13.3 reduce-scatter.2
  216.6 74.2 all-gather.17
  293.1 72.8 all-gather.15
  368.1 76.2 all-gather.19
  450.9 12.7 reduce-scatter.4
where the time goes:
time: 473 us; the launch traced here: 472 us
  waiting for transfers between devices  329 us (70%)
  blocking collectives  60.3 us (13%)
  matrix products  32.2 us (7%)
  local copies, waits for them, and re-layouts  22.4 us (5%)
  between operations  13.5 us (3%)
  other arithmetic  12.6 us (3%)
    all_gather x1, waiting for transfers between devices, body(): lax.all_gather(w_gate, 'sp', axis=0, tiled=True)  70.4 us
    all_gather x1, waiting for transfers between devices, body(): lax.all_gather(w_down, 'sp', axis=1, tiled=True)  68.5 us
    all_gather x1, waiting for transfers between devices, body(): lax.all_gather(w_up, 'sp', axis=0, tiled=True)  65.4 us
    all_gather x1, waiting for transfers between devices, body(): keys_l = lax.all_gather(k_large, 'sp', axis=0, tiled=True)  38 us
    all_gather x1, waiting for transfers between devices, body(): keys_s = lax.all_gather(k_small, 'sp', axis=0, tiled=True)  31.4 us
    all_gather x1, blocking collectives, body(): lax.all_gather(local_large, 'sp', axis=0, tiled=True)  27.1 us
    all_gather x1, waiting for transfers between devices, body(): values_s = lax.all_gather(v_small, 'sp', axis=0, tiled=True)  26 us
    all_gather x1, blocking collectives, body(): lax.all_gather(local_small, 'sp', axis=0, tiled=True)  24.5 us
  transfers between devices with their start and end apart: 10, of which 9 were waited for; matrix products, arithmetic and copies ran while one was open for 9% of the time, Pallas kernels for 0%

commit v1 on v0

--- a/solution.py
+++ b/solution.py
@@ -104,8 +104,11 @@
         empty_carry(rows, heads_small, queries_small.shape[2]),
         empty_carry(rows, heads_large, queries_large.shape[2]),
     )
-    keys_s = lax.all_gather(k_small, "sp", axis=0, tiled=True)
-    values_s = lax.all_gather(v_small, "sp", axis=0, tiled=True)
+    keys_s, values_s = jnp.split(
+        lax.all_gather(jnp.concatenate([k_small, v_small], axis=1), "sp", axis=0, tiled=True),
+        [k_small.shape[1]],
+        axis=1,
+    )
     keys_l = lax.all_gather(k_large, "sp", axis=0, tiled=True)
     values_l = lax.all_gather(v_large, "sp", axis=0, tiled=True)
     small = attend(start_carry[0], keys_s, values_s, queries_small, cum_small, every_small, qpos)

time: 473 us -> 459 us (0.970)
  waiting for transfers between devices: 329 us -> 311 us
    split x0 -> x3, local copies, waits for them, and re-layouts: none -> 12.5 us  [body(): jnp.split(lax.all_gather(jnp.concatenate([k_small, v_small], axis=1), 'sp...]
    all_gather x2 -> x1, waiting for transfers between devices: 57.4 us -> 45.2 us  [body(): lax.all_gather(jnp.concatenate([k_small, v_small], axis=1), 'sp', axis=0,...]
    all_gather x2 -> x0, local copies, waits for them, and re-layouts: 7.94 us -> none  [the longest x1 4 us: body(): keys_s = lax.all_gather(k_small, 'sp', axis=0, tiled=True)]
  transfers between devices with their start and end apart: 10 -> 9, of which waited for: 9 -> 8; matrix products, arithmetic and copies ran while one was open for 9% -> 6% of each run, Pallas kernels for 0% -> 0%
where the time goes in v1:
time: 459 us; the launch traced here: 458 us
  waiting for transfers between devices  311 us (68%)
  blocking collectives  59.4 us (13%)
  matrix products  33.7 us (7%)
  local copies, waits for them, and re-layouts  21.2 us (5%)
  other arithmetic  16.8 us (4%)
  between operations  13.8 us (3%)
    all_gather x1, waiting for transfers between devices, body(): lax.all_gather(w_gate, 'sp', axis=0, tiled=True)  70.3 us
    all_gather x1, waiting for transfers between devices, body(): lax.all_gather(w_down, 'sp', axis=1, tiled=True)  68.5 us
    all_gather x1, waiting for transfers between devices, body(): lax.all_gather(w_up, 'sp', axis=0, tiled=True)  65.4 us
    all_gather x1, waiting for transfers between devices, body(): lax.all_gather(jnp.concatenate([k_small, v_small], axis=1), 'sp', axis=0,...  45.2 us
    all_gather x1, waiting for transfers between devices, body(): keys_l = lax.all_gather(k_large, 'sp', axis=0, tiled=True)  33.9 us
    all_gather x1, blocking collectives, body(): lax.all_gather(local_large, 'sp', axis=0, tiled=True)  26.7 us
    all_gather x1, blocking collectives, body(): lax.all_gather(local_small, 'sp', axis=0, tiled=True)  24 us
    reduce_scatter x1, waiting for transfers between devices, body(): lax.psum_scatter(jnp.dot(hidden, down_full, preferred_element_type=jnp.fl...  13 us
  transfers between devices with their start and end apart: 9, of which 8 were waited for; matrix products, arithmetic and copies ran while one was open for 6% of the time, Pallas kernels for 0%

profile of v1, /device:TPU:0, one launch (start us, length us, event | category | flops | bytes accessed | tf_op | source)
XLA Modules:
  0.0 458.2 jit_solution(5734372286156607428)
XLA Ops:
  6.5 0.7 all-gather.11.cloned.1.call-update
  7.3 0.0 all-gather.9.cloned.1.call-start
  7.3 1.7 copy.44
  9.0 0.0 all-gather.9.cloned.1.call-update
  9.0 0.0 all-gather.7.cloned.1.call-start
  9.0 1.7 pad_maximum_fusion
  10.7 0.0 all-gather.7.cloned.1.call-update
  10.8 0.0 reduce-scatter.3.cloned.1.call-start
  10.8 0.7 fusion.40
  11.5 0.1 copy.47
  11.6 0.2 reduce_window_sum.46
  11.8 26.7 %all_gather.30 = f32[2048,4]{1,0:T(8,128)S(1)} all-gather(f32[128,4]{1,0:T(8,128)S(1)} %reduce_window_sum.46), channel_id=1, replica_groups=mesh['sp'=16,'tp'=2] {'sp'}, dimensions={0}, use_global_device_ids=true | all-gather | bytes 34816 | tf_op jit(solution)/shard_map/all_gather | solution.py:93
  38.5 0.1 bitcast_add_fusion.2
  38.6 0.1 copy.50
  38.7 0.3 copy.51
  39.1 0.1 copy.38
  39.2 0.2 reduce_window_sum.44
  39.4 24.0 %all_gather.28 = f32[2048,8]{1,0:T(8,128)S(1)} all-gather(f32[128,8]{1,0:T(8,128)S(1)} %reduce_window_sum.44), channel_id=1, replica_groups=mesh['sp'=16,'tp'=2] {'sp'}, dimensions={0}, use_global_device_ids=true | all-gather | bytes 69632 | tf_op jit(solution)/shard_map/all_gather | solution.py:92
  63.4 0.1 bitcast_add_fusion.3
  63.5 0.3 copy.42
  63.8 0.1 copy.37
  64.0 0.2 iota_compare_fusion
  64.1 0.0 all-gather.11.cloned.1.call-done
  64.2 4.0 copy.52
  68.2 33.9 %all-gather.9.cloned.1.call-done = bf16[2048,512]{0,1:T(8,128)(2,1)} async-done(((bf16[128,512]{0,1:T(8,128)(2,1)}), bf16[2048,512]{0,1:T(8,128)(2,1)}) %all-gather.9.cloned.1.call-update) | async-done | bytes 2097168 | tf_op jit(solution)/shard_map/all_gather | solution.py:112
  102.1 3.7 fusion.48
  105.8 0.8 fusion.10
  106.5 0.8 copy-done.6
  107.3 1.2 multiply_reduce_fusion.1
  108.6 45.2 %all-gather.7.cloned.1.call-done = bf16[2048,1024]{1,0:T(8,128)(2,1)} async-done(((bf16[128,1024]{1,0:T(8,128)(2,1)}), bf16[2048,1024]{1,0:T(8,128)(2,1)}) %all-gather.7.cloned.1.call-update) | async-done | bytes 4194320 | tf_op jit(solution)/shard_map/all_gather | solution.py:108
  153.7 4.6 fusion.46
  158.3 3.9 copy.36
  162.2 6.7 %fusion.4 = (f32[128,8]{0,1:T(8,128)S(1)}, f32[8,2048,128]{2,1,0:T(8,128)}) fusion(f32[8,2048]{1,0:T(8,128)S(1)} %copy.42, f32[128,8]{0,1:T(8,128)S(1)} %copy.41, pred[128,2048]{0,1:T(8,128)(4,1)S(1)} %iota_compare_fusion, bf16[2048,8,64]{0,2,1:T(8,128)(2,1)} %bitcast.82, bf16[128,8,64]{0,2,1:T(8,128)(2,1)S(1)} %bitcast.85), kind=kOutput, calls=%fused_computation.6 | convolution fusion | flops 278920192 | bytes 10952704 | tf_op jit(solution)/shard_map/qhd,khd->qhk/dot_general | solution.py:32
  168.9 3.9 copy.35
  172.8 6.6 %fusion.2 = f32[128,8]{0,1:T(8,128)S(1)} fusion(f32[8,2048,128]{2,1,0:T(8,128)} %get-tuple-element.11, f32[128,8]{0,1:T(8,128)S(1)} %broadcast_maximum_fusion, f32[8,2048]{1,0:T(8,128)S(1)} %copy.42, f32[128,8]{0,1:T(8,128)S(1)} %copy.41, pred[128,2048]{0,1:T(8,128)(4,1)S(1)} %iota_compare_fusion), kind=kLoop, calls=%fused_computation.4 | loop fusion | flops 14679040 | bytes 8728576 | tf_op jit(solution)/shard_map/reduce_sum | solution.py:40
  179.5 4.8 %multiply_reduce_fusion.2 = (f32[128,8]{0,1:T(8,128)S(1)}, f32[128,8,64]{0,2,1:T(8,128)S(1)}) fusion(f32[128,8]{0,1:T(8,128)S(1)} %fusion.2, bf16[2048,8,64]{0,2,1:T(8,128)(2,1)} %bitcast.81, f32[8,2048,128]{2,1,0:T(8,128)S(1)} %copy-done.2, f32[128,8]{0,1:T(8,128)S(1)} %broadcast_maximum_fusion, f32[8,2048]{1,0:T(8,128)S(1)} %copy.42, ...), kind=kOutput, calls=%fused_computation.50 | convolution fusion | flops 283311104 | bytes 11091968 | tf_op jit(solution)/shard_map/qhk,khd->qhd/dot_general | solution.py:41
  184.5 0.5 fusion.49
  184.9 1.0 copy-done.5
  185.9 1.3 fusion.12
  187.3 0.0 reduce-scatter.3.cloned.1.call-update
  187.3 0.0 all-gather.15.cloned.1.call-start
  187.3 0.5 all-gather.15.cloned.1.call-update
  187.9 0.0 all-gather.13.cloned.1.call-start
  187.9 0.5 all-gather.13.cloned.1.call-update
  188.4 0.0 all-gather.17.cloned.1.call-start
  188.5 0.7 all-gather.17.cloned.1.call-update
  189.2 0.0 reduce-scatter.5.cloned.1.call-start
  189.3 11.3 %reduce-scatter.3.cloned.1.call-done = bf16[64,2048]{1,0:T(8,128)(2,1)} async-done(((bf16[128,2048]{1,0:T(8,128)(2,1)}), bf16[64,2048]{1,0:T(8,128)(2,1)}) %reduce-scatter.3.cloned.1.call-update) | async-done | bytes 262160 | tf_op jit(solution)/shard_map/reduce_scatter | solution.py:119
  200.6 1.1 multiply_reduce_fusion
  201.8 1.1 multiply_convert_fusion
  202.8 8.7 %all_gather.32 = bf16[128,2048]{1,0:T(8,128)(2,1)S(1)} all-gather(bf16[64,2048]{1,0:T(8,128)(2,1)S(1)} %multiply_convert_fusion), channel_id=1, replica_groups=mesh['sp'=16,'tp'=2] {'tp'}, dimensions={0}, use_global_device_ids=true | all-gather | bytes 786432 | tf_op jit(solution)/shard_map/all_gather | solution.py:132
  211.5 65.4 %all-gather.15.cloned.1.call-done = bf16[2048,2048]{1,0:T(8,128)(2,1)} async-done(((bf16[128,2048]{1,0:T(8,128)(2,1)}), bf16[2048,2048]{1,0:T(8,128)(2,1)}) %all-gather.15.cloned.1.call-update) | async-done | bytes 8388624 | tf_op jit(solution)/shard_map/all_gather | solution.py:86
  276.9 4.6 %convolution_convert_fusion.1 = bf16[128,2048]{1,0:T(8,128)(2,1)S(1)} fusion(bf16[128,2048]{1,0:T(8,128)(2,1)S(1)} %all_gather.32, bf16[2048,2048]{1,0:T(8,128)(2,1)} %all-gather.15.cloned.1.call-done), kind=kOutput, calls=%fused_computation.17 | convolution fusion | flops 1074003968 | bytes 9437184 | tf_op jit(solution)/shard_map/dot_general | solution.py:134
  281.6 70.3 %all-gather.13.cloned.1.call-done = bf16[2048,2048]{1,0:T(8,128)(2,1)} async-done(((bf16[128,2048]{1,0:T(8,128)(2,1)}), bf16[2048,2048]{1,0:T(8,128)(2,1)}) %all-gather.13.cloned.1.call-update) | async-done | bytes 8388624 | tf_op jit(solution)/shard_map/all_gather | solution.py:85
  351.9 4.6 %convolution_convert_fusion.2 = bf16[128,2048]{1,0:T(8,128)(2,1)S(1)} fusion(bf16[128,2048]{1,0:T(8,128)(2,1)S(1)} %all_gather.32, bf16[2048,2048]{1,0:T(8,128)(2,1)} %all-gather.13.cloned.1.call-done), kind=kOutput, calls=%fused_computation.18 | convolution fusion | flops 1074003968 | bytes 9437184 | tf_op jit(solution)/shard_map/dot_general | solution.py:133
  356.5 2.2 collective-permute-start
  358.7 0.8 collective-permute-done
  359.5 0.3 maximum_convert_fusion
  359.8 2.0 fusion.15
  361.8 68.5 %all-gather.17.cloned.1.call-done = bf16[2048,2048]{1,0:T(8,128)(2,1)} async-done(((bf16[2048,128]{1,0:T(8,128)(2,1)}), bf16[2048,2048]{1,0:T(8,128)(2,1)}) %all-gather.17.cloned.1.call-update) | async-done | bytes 8388624 | tf_op jit(solution)/shard_map/all_gather | solution.py:87
  430.3 6.3 %convolution_convert_fusion = bf16[128,2048]{1,0:T(8,128)(2,1)} fusion(bf16[2048,2048]{1,0:T(8,128)(2,1)} %all-gather.17.cloned.1.call-done, f32[128,4096]{1,0:T(8,128)} %fusion.15), kind=kOutput, calls=%fused_computation.16 | convolution fusion | flops 1075576832 | bytes 11010048 | tf_op jit(solution)/shard_map/dot_general | solution.py:148
  436.7 0.0 reduce-scatter.5.cloned.1.call-update
  436.7 13.0 %reduce-scatter.5.cloned.1.call-done = bf16[64,2048]{1,0:T(8,128)(2,1)} async-done(((bf16[128,2048]{1,0:T(8,128)(2,1)}), bf16[64,2048]{1,0:T(8,128)(2,1)}) %reduce-scatter.5.cloned.1.call-update) | async-done | bytes 262160 | tf_op jit(solution)/shard_map/reduce_scatter | solution.py:147
  449.6 1.7 add_convert_fusion
  (43 shorter events, 0.4 us)
Async XLA Ops:
  6.5 177.9 %copy-start = (bf16[512,2048]{1,0:T(8,128)(2,1)S(1)}, bf16[512,2048]{1,0:T(8,128)(2,1)}, u32[]{:S(2)}) copy-start(bf16[512,2048]{1,0:T(8,128)(2,1)} %param.26) | copy-start | bytes 6291460
  6.5 32.5 %copy-start.11 = (f32[128,8]{0,1:T(8,128)S(1)}, f32[128,8]{0,1:T(8,128)}, u32[]{:S(2)}) copy-start(f32[128,8]{0,1:T(8,128)} %param.24) | copy-start | bytes 12292
  6.5 57.6 %all-gather.11.cloned.1.call-start = ((), (), s32[]{:S(2)}) async-start(), calls=%async_computation.4 | async-start | bytes 2228224 | tf_op jit(solution)/shard_map/all_gather | solution.py:113
  7.3 94.8 %all-gather.9.cloned.1.call-start = ((), (), s32[]{:S(2)}) async-start(), calls=%async_computation.3 | async-start | bytes 2228224 | tf_op jit(solution)/shard_map/all_gather | solution.py:112
  9.0 144.7 %all-gather.7.cloned.1.call-start = ((), (), s32[]{:S(2)}) async-start(), calls=%async_computation.2 | async-start | bytes 4456448 | tf_op jit(solution)/shard_map/all_gather | solution.py:108
  10.8 189.8 %reduce-scatter.3.cloned.1.call-start = ((), (), s32[]{:S(2)}) async-start(), calls=%async_computation.5 | async-start | bytes 786432 | tf_op jit(solution)/shard_map/reduce_scatter | solution.py:119
  38.5 25.3 %copy-start.7 = (bf16[128,512]{1,0:T(8,128)(2,1)S(1)}, bf16[128,512]{1,0:T(8,128)(2,1)}, u32[]{:S(2)}) copy-start(bf16[128,512]{1,0:T(8,128)(2,1)} %param.18) | copy-start | bytes 393220
  63.3 38.7 %copy-start.12 = (bf16[128,512]{1,0:T(8,128)(2,1)S(1)}, bf16[128,512]{1,0:T(8,128)(2,1)}, u32[]{:S(2)}) copy-start(bf16[128,512]{1,0:T(8,128)(2,1)} %param.21) | copy-start | bytes 393220
  105.8 1.6 copy-start.6
  172.8 6.6 %copy-start.2 = (f32[8,2048,128]{2,1,0:T(8,128)S(1)}, f32[8,2048,128]{2,1,0:T(8,128)}, u32[]{:S(2)}) copy-start(f32[8,2048,128]{2,1,0:T(8,128)} %get-tuple-element.11) | copy-start | bytes 25165828
  184.4 1.6 copy-start.5
  184.4 4.8 %copy-start.8 = (f32[3,2048]{1,0:T(4,128)S(1)}, f32[3,2048]{1,0:T(4,128)}, u32[]{:S(2)}) copy-start(f32[3,2048]{1,0:T(4,128)} %param.31) | copy-start | bytes 73732
  184.4 4.8 %copy-start.9 = (f32[3,2048]{1,0:T(4,128)S(1)}, f32[3,2048]{1,0:T(4,128)}, u32[]{:S(2)}) copy-start(f32[3,2048]{1,0:T(4,128)} %param.32) | copy-start | bytes 73732
  184.4 16.2 %copy-start.3 = (bf16[64,2048]{1,0:T(8,128)(2,1)S(1)}, bf16[64,2048]{1,0:T(8,128)(2,1)}, u32[]{:S(2)}) copy-start(bf16[64,2048]{1,0:T(8,128)(2,1)} %param.17) | copy-start | bytes 786436
  184.5 17.3 %copy-start.10 = (f32[2048]{0:T(1024)S(1)}, f32[2048]{0:T(1024)}, u32[]{:S(2)}) copy-start(f32[2048]{0:T(1024)} %param.28) | copy-start | bytes 24580
  187.3 89.6 %all-gather.15.cloned.1.call-start = ((), (), s32[]{:S(2)}) async-start(), calls=%async_computation.7 | async-start | bytes 8912896 | tf_op jit(solution)/shard_map/all_gather | solution.py:86
  187.9 164.0 %all-gather.13.cloned.1.call-start = ((), (), s32[]{:S(2)}) async-start(), calls=%async_computation.6 | async-start | bytes 8912896 | tf_op jit(solution)/shard_map/all_gather | solution.py:85
  188.4 241.9 %all-gather.17.cloned.1.call-start = ((), (), s32[]{:S(2)}) async-start(), calls=%async_computation.8 | async-start | bytes 8912896 | tf_op jit(solution)/shard_map/all_gather | solution.py:87
  189.2 260.4 %reduce-scatter.5.cloned.1.call-start = ((), (), s32[]{:S(2)}) async-start(), calls=%async_computation.9 | async-start | bytes 786432 | tf_op jit(solution)/shard_map/reduce_scatter | solution.py:147
  356.5 3.0 collective-permute-start
  361.8 87.8 %copy-start.4 = (bf16[64,2048]{1,0:T(8,128)(2,1)S(1)}, bf16[64,2048]{1,0:T(8,128)(2,1)}, u32[]{:S(2)}) copy-start(bf16[64,2048]{1,0:T(8,128)(2,1)} %reduce-scatter.3.cloned.1.call-done) | copy-start | bytes 786436
  430.3 21.0 %copy-start.1 = (bf16[512,2048]{1,0:T(8,128)(2,1)S(1)}, bf16[512,2048]{1,0:T(8,128)(2,1)}, u32[]{:S(2)}) copy-start(bf16[512,2048]{1,0:T(8,128)(2,1)} %param.26) | copy-start | bytes 6291460
Sparse Core Ops, SparseCore 0:
  9.5 49.8 all-gather.10
  61.6 40.4 all-gather.8
  104.2 49.4 all-gather.6
  187.4 13.1 reduce-scatter.2
  202.6 74.2 all-gather.14
  278.9 72.8 all-gather.12
  354.0 76.2 all-gather.16
  436.8 12.7 reduce-scatter.4
